TPU v7x, 32 devices: a whole 2x2x4 slice. The times are simulated.
32 devices in a mesh: fs: 8 (over z, y), tp: 4 (over x, core).
Axes of the slice: x: 2, y: 2, z: 4, core: 2. Of those that a mesh axis runs over, the one named last changes fastest.
Arguments:
- normed_input: bfloat16 [8192, 4096], P('fs'), may hold values from -6 to 6
- query_cotangent: bfloat16 [8192, 2048], P('fs', 'tp'), may hold values from -40 to 40
- key_cotangent: bfloat16 [8192, 2048], P('fs', 'tp'), may hold values from -40 to 40
- head_outputs: bfloat16 [8192, 2048], P('fs', 'tp'), may hold values from -40 to 40
- output_cotangent: bfloat16 [8192, 4096], P('fs'), may hold values from -6 to 6
- query_basis: bfloat16 [4096, 256], P('fs'), may hold values from -2.5 to 2.5
- key_basis: bfloat16 [4096, 256], P('fs'), may hold values from -2.5 to 2.5
- output_basis: bfloat16 [4096, 256], P('fs'), may hold values from -2.5 to 2.5
- query_master: float32 [4096, 2048], P('fs', 'tp'), may hold values from -6 to 6
- key_master: float32 [4096, 2048], P('fs', 'tp'), may hold values from -6 to 6
- output_master: float32 [2048, 4096], P('tp', 'fs'), may hold values from -6 to 6
- query_first: float32 [256, 2048], P('fs', 'tp'), may hold values from -6 to 6
- query_second: float32 [256, 2048], P('fs', 'tp'), may hold values from 0.05 to 0.5
- key_first: float32 [256, 2048], P('fs', 'tp'), may hold values from -6 to 6
- key_second: float32 [256, 2048], P('fs', 'tp'), may hold values from 0.05 to 0.5
- output_first: float32 [256, 2048], P('fs', 'tp'), may hold values from -6 to 6
- output_second: float32 [256, 2048], P('fs', 'tp'), may hold values from 0.05 to 0.5
Outputs:
- query_master_new: float32 [4096, 2048], P('fs', 'tp')
- key_master_new: float32 [4096, 2048], P('fs', 'tp')
- output_master_new: float32 [2048, 4096], P('tp', 'fs')
- query_copy: bfloat16 [4096, 2048], P(None, 'tp')
- key_copy: bfloat16 [4096, 2048], P(None, 'tp')
- output_copy: bfloat16 [2048, 4096], P('tp')
- query_step: bfloat16 [4096, 2048], P('fs', 'tp')
- key_step: bfloat16 [4096, 2048], P('fs', 'tp')
- output_step: bfloat16 [2048, 4096], P('tp', 'fs')
- query_first_new: float32 [256, 2048], P('fs', 'tp')
- query_second_new: float32 [256, 2048], P('fs', 'tp')
- key_first_new: float32 [256, 2048], P('fs', 'tp')
- key_second_new: float32 [256, 2048], P('fs', 'tp')
- output_first_new: float32 [256, 2048], P('fs', 'tp')
- output_second_new: float32 [256, 2048], P('fs', 'tp')
All inputs are finite; a program needn't handle non-finite values.
Results may differ from a plain program's by a relative error of at most 0.007.
Values may be sent and summed in bfloat16 or wider, within the bound.
A program may use at most 128 MiB of HBM per device.

v0:
```python
import jax
import jax.numpy as jnp
from jax import lax
from jax.sharding import PartitionSpec as P

RANK = 256
C_W = 2048


bias_first = 1.0 / (1.0 - 0.8**10)
bias_second = 1.0 / (1.0 - 0.95**10)
learn_rate = 0.05
decay_rate = 0.1


def split_product(reduced, right_side):
    upper = reduced.astype(jnp.bfloat16)
    lower = (reduced - upper.astype(jnp.float32)).astype(jnp.bfloat16)
    first_part = jnp.einsum("tr,tc->rc", upper, right_side, preferred_element_type=jnp.float32)
    second_part = jnp.einsum("tr,tc->rc", lower, right_side, preferred_element_type=jnp.float32)
    return first_part + second_part


def body(
    normed_input,
    query_cotangent,
    key_cotangent,
    head_outputs,
    output_cotangent,
    query_basis,
    key_basis,
    output_basis,
    query_master,
    key_master,
    output_master,
    query_first,
    query_second,
    key_first,
    key_second,
    output_first,
    output_second,
):
    width = query_cotangent.shape[1]
    bases = (query_basis, key_basis, output_basis)
    reduced = (
        jnp.dot(
            normed_input,
            lax.all_gather(query_basis, "fs", axis=0, tiled=True),
            preferred_element_type=jnp.float32,
        ),
        jnp.dot(
            normed_input,
            lax.all_gather(key_basis, "fs", axis=0, tiled=True),
            preferred_element_type=jnp.float32,
        ),
        jnp.dot(
            output_cotangent,
            lax.all_gather(output_basis, "fs", axis=0, tiled=True),
            preferred_element_type=jnp.float32,
        ),
    )
    right_sides = (query_cotangent, key_cotangent, head_outputs)
    partial_value = jnp.concatenate(
        [split_product(reduced[member], right_sides[member]) for member in range(3)], axis=1
    )
    shares = lax.psum_scatter(partial_value, "fs", scatter_dimension=0, tiled=True)
    sum_squares = lax.psum(jnp.sum(shares * shares), ("fs", "tp"))
    clip_factor = jnp.minimum(1.0, jnp.sqrt(3.0 * RANK * C_W / sum_squares))
    clipped = clip_factor * shares
    first_moment = jnp.concatenate([query_first, key_first, output_first], axis=1)
    second_moment = jnp.concatenate([query_second, key_second, output_second], axis=1)
    first_new = 0.8 * first_moment + 0.2 * clipped
    second_new = 0.95 * second_moment + 0.05 * clipped * clipped
    direction = (first_new * bias_first / (jnp.sqrt(second_new * bias_second) + 1e-08)).astype(
        jnp.bfloat16
    )
    portion = lax.all_gather(direction, "fs", axis=0, tiled=True)
    result = []
    for member in range(3):
        columns = bases[member]
        result.append(
            jnp.dot(
                columns,
                portion[:, member * width : (member + 1) * width],
                preferred_element_type=jnp.float32,
            )
        )
    updates = tuple(result)
    query_update = 0.25 * updates[0]
    key_update = 0.25 * updates[1]
    output_update = 0.25 * updates[2].T
    query_master_new = query_master - learn_rate * (query_update + decay_rate * query_master)
    key_master_new = key_master - learn_rate * (key_update + decay_rate * key_master)
    output_master_new = output_master - learn_rate * (output_update + decay_rate * output_master)
    query_copy, key_copy, output_copy = (
        lax.all_gather(query_master_new.astype(jnp.bfloat16), "fs", axis=0, tiled=True),
        lax.all_gather(key_master_new.astype(jnp.bfloat16), "fs", axis=0, tiled=True),
        lax.all_gather(output_master_new.astype(jnp.bfloat16), "fs", axis=1, tiled=True),
    )
    return (
        query_master_new,
        key_master_new,
        output_master_new,
        query_copy,
        key_copy,
        output_copy,
        query_update.astype(jnp.bfloat16),
        key_update.astype(jnp.bfloat16),
        output_update.astype(jnp.bfloat16),
        first_new[:, :width],
        second_new[:, :width],
        first_new[:, width : 2 * width],
        second_new[:, width : 2 * width],
        first_new[:, 2 * width :],
        second_new[:, 2 * width :],
    )


def solution(mesh):
    placed = (
        P("fs", None),
        P("fs", "tp"),
        P("fs", "tp"),
        P("fs", "tp"),
        P("fs", None),
        P("fs", None),
        P("fs", None),
        P("fs", None),
        P("fs", "tp"),
        P("fs", "tp"),
        P("tp", "fs"),
        P("fs", "tp"),
        P("fs", "tp"),
        P("fs", "tp"),
        P("fs", "tp"),
        P("fs", "tp"),
        P("fs", "tp"),
    )
    return jax.shard_map(
        body,
        mesh=mesh,
        in_specs=placed,
        out_specs=(
            P("fs", "tp"),
            P("fs", "tp"),
            P("tp", "fs"),
            P(None, "tp"),
            P(None, "tp"),
            P("tp", None),
            P("fs", "tp"),
            P("fs", "tp"),
            P("tp", "fs"),
            P("fs", "tp"),
            P("fs", "tp"),
            P("fs", "tp"),
            P("fs", "tp"),
            P("fs", "tp"),
            P("fs", "tp"),
        ),
        check_vma=False,
    )
```

profile of v0, /device:TPU:0, one launch (start us, length us, event | category | flops | bytes accessed | tf_op | source)
XLA Modules:
  0.0 548.4 jit_solution(1708775722781414936)
XLA Ops:
  9.5 52.5 %all-gather.11.cloned.1.call-done = bf16[4096,256]{1,0:T(8,128)(2,1)} async-done(((bf16[512,256]{1,0:T(8,128)(2,1)}), bf16[4096,256]{1,0:T(8,128)(2,1)}) %all-gather.11.cloned.1.call-update) | async-done | bytes 2097168 | tf_op jit(solution)/shard_map/all_gather | solution.py:58
  62.0 6.3 %fusion.26 = f32[1024,256]{1,0:T(8,128)S(1)} fusion(bf16[1024,4096]{1,0:T(8,128)(2,1)} %param.21, bf16[4096,256]{1,0:T(8,128)(2,1)} %all-gather.11.cloned.1.call-done), kind=kOutput, calls=%fused_computation.42 | convolution fusion | flops 2147483648 | bytes 11534336 | tf_op jit(solution)/shard_map/dot_general | solution.py:56
  69.6 42.2 %all-gather.9.cloned.1.call-done = bf16[4096,256]{1,0:T(8,128)(2,1)} async-done(((bf16[512,256]{1,0:T(8,128)(2,1)}), bf16[4096,256]{1,0:T(8,128)(2,1)}) %all-gather.9.cloned.1.call-update) | async-done | bytes 2097168 | tf_op jit(solution)/shard_map/all_gather | solution.py:53
  111.8 6.3 %fusion.25 = f32[1024,256]{1,0:T(8,128)S(1)} fusion(bf16[1024,4096]{1,0:T(8,128)(2,1)} %param.17, bf16[4096,256]{1,0:T(8,128)(2,1)} %all-gather.9.cloned.1.call-done), kind=kOutput, calls=%fused_computation.41 | convolution fusion | flops 2147483648 | bytes 11534336 | tf_op jit(solution)/shard_map/dot_general | solution.py:51
  121.0 40.7 %all-gather.7.cloned.1.call-done = bf16[4096,256]{1,0:T(8,128)(2,1)} async-done(((bf16[512,256]{1,0:T(8,128)(2,1)}), bf16[4096,256]{1,0:T(8,128)(2,1)}) %all-gather.7.cloned.1.call-update) | async-done | bytes 2097168 | tf_op jit(solution)/shard_map/all_gather | solution.py:48
  161.7 6.3 %fusion.24 = f32[1024,256]{1,0:T(8,128)S(1)} fusion(bf16[1024,4096]{1,0:T(8,128)(2,1)} %param.17, bf16[4096,256]{1,0:T(8,128)(2,1)} %all-gather.7.cloned.1.call-done), kind=kOutput, calls=%fused_computation.40 | convolution fusion | flops 2147483648 | bytes 11534336 | tf_op jit(solution)/shard_map/dot_general | solution.py:46
  170.9 64.1 %reduce-scatter.2.cloned.1.call-done = f32[32,1536]{1,0:T(8,128)} async-done(((f32[256,1536]{1,0:T(8,128)}), f32[32,1536]{1,0:T(8,128)}) %reduce-scatter.2.cloned.1.call-update) | async-done | bytes 196624 | tf_op jit(solution)/shard_map/reduce_scatter | solution.py:66
  235.1 1.7 multiply_reduce_fusion
  237.1 39.7 %psum.7 = f32[]{:T(128)} all-reduce(f32[]{:T(128)} %multiply_reduce_fusion), channel_id=1, replica_groups=mesh['fs'=8,'tp'=4] {'fs','tp'}, use_global_device_ids=true, to_apply=%region_2.0 | all-reduce | flops 1 | bytes 8 | tf_op jit(solution)/shard_map/psum | solution.py:67
  278.5 32.1 %all_gather.24 = bf16[256,1536]{1,0:T(8,128)(2,1)S(1)} all-gather(bf16[32,1536]{1,0:T(8,128)(2,1)S(1)} %get-tuple-element.36), channel_id=1, replica_groups=mesh['fs'=8,'tp'=4] {'fs'}, dimensions={0}, use_global_device_ids=true | all-gather | bytes 884736 | tf_op jit(solution)/shard_map/all_gather | solution.py:77
  310.6 1.4 fusion.17
  312.1 1.6 copy.33
  313.6 2.4 fusion.18
  316.3 2.5 copy.38
  318.8 2.1 fusion.23
  322.2 2.6 fusion.16
  324.9 2.0 copy.46
  328.2 2.0 copy.45
  333.6 53.0 %all-gather.15.cloned.1.call-done = bf16[4096,512]{0,1:T(8,128)(2,1)} async-done(((bf16[512,512]{0,1:T(8,128)(2,1)}), bf16[4096,512]{0,1:T(8,128)(2,1)}) %all-gather.15.cloned.1.call-update) | async-done | bytes 4194320 | tf_op jit(solution)/shard_map/all_gather | solution.py:97
  386.7 6.4 %copy.43 = bf16[4096,512]{1,0:T(8,128)(2,1)} copy(bf16[4096,512]{0,1:T(8,128)(2,1)} %all-gather.15.cloned.1.call-done) | data formatting | bytes 8388608
  393.1 68.9 %all-gather.13.cloned.1.call-done = bf16[4096,512]{0,1:T(8,128)(2,1)} async-done(((bf16[512,512]{0,1:T(8,128)(2,1)}), bf16[4096,512]{0,1:T(8,128)(2,1)}) %all-gather.13.cloned.1.call-update) | async-done | bytes 4194320 | tf_op jit(solution)/shard_map/all_gather | solution.py:96
  462.0 6.4 %copy.42 = bf16[4096,512]{1,0:T(8,128)(2,1)} copy(bf16[4096,512]{0,1:T(8,128)(2,1)} %all-gather.13.cloned.1.call-done) | data formatting | bytes 8388608
  468.4 66.7 %all-gather.17.cloned.1.call-done = bf16[512,4096]{0,1:T(8,128)(2,1)} async-done(((bf16[512,512]{0,1:T(8,128)(2,1)}), bf16[512,4096]{0,1:T(8,128)(2,1)}) %all-gather.17.cloned.1.call-update) | async-done | bytes 4194320 | tf_op jit(solution)/shard_map/all_gather | solution.py:98
  535.1 6.4 %copy.44 = bf16[512,4096]{1,0:T(8,128)(2,1)} copy(bf16[512,4096]{0,1:T(8,128)(2,1)} %all-gather.17.cloned.1.call-done) | data formatting | bytes 8388608
  (68 shorter events, 16.6 us)
Async XLA Ops:
  7.2 61.1 %copy-start = (bf16[1024,512]{1,0:T(8,128)(2,1)S(1)}, bf16[1024,512]{1,0:T(8,128)(2,1)}, u32[]{:S(2)}) copy-start(bf16[1024,512]{1,0:T(8,128)(2,1)} %param.20) | copy-start | bytes 3145732
  7.2 54.8 %all-gather.11.cloned.1.call-start = ((), (), s32[]{:S(2)}) async-start(), calls=%async_computation.3 | async-start | bytes 2359296 | tf_op jit(solution)/shard_map/all_gather | solution.py:58
  7.9 103.9 %all-gather.9.cloned.1.call-start = ((), (), s32[]{:S(2)}) async-start(), calls=%async_computation.2 | async-start | bytes 2359296 | tf_op jit(solution)/shard_map/all_gather | solution.py:53
  8.7 153.0 %all-gather.7.cloned.1.call-start = ((), (), s32[]{:S(2)}) async-start(), calls=%async_computation.1 | async-start | bytes 2359296 | tf_op jit(solution)/shard_map/all_gather | solution.py:48
  9.4 225.6 %reduce-scatter.2.cloned.1.call-start = ((), (), s32[]{:S(2)}) async-start(), calls=%async_computation.4 | async-start | bytes 1769472 | tf_op jit(solution)/shard_map/reduce_scatter | solution.py:66
  69.6 48.6 %copy-start.2 = (bf16[1024,512]{1,0:T(8,128)(2,1)S(1)}, bf16[1024,512]{1,0:T(8,128)(2,1)}, u32[]{:S(2)}) copy-start(bf16[1024,512]{1,0:T(8,128)(2,1)} %param.19) | copy-start | bytes 3145732
  120.9 47.1 %copy-start.3 = (bf16[1024,512]{1,0:T(8,128)(2,1)S(1)}, bf16[1024,512]{1,0:T(8,128)(2,1)}, u32[]{:S(2)}) copy-start(bf16[1024,512]{1,0:T(8,128)(2,1)} %param.18) | copy-start | bytes 3145732
  169.5 67.2 %copy-start.9 = (f32[512,512]{1,0:T(8,128)S(1)}, f32[512,512]{1,0:T(8,128)}, u32[]{:S(2)}) copy-start(f32[512,512]{1,0:T(8,128)} %param.26) | copy-start | bytes 3145732
  170.8 106.7 %copy-start.14 = (f32[32,512]{1,0:T(8,128)S(1)}, f32[32,512]{1,0:T(8,128)}, u32[]{:S(2)}) copy-start(f32[32,512]{1,0:T(8,128)} %param.32) | copy-start | bytes 196612
  170.8 106.7 %copy-start.15 = (f32[32,512]{1,0:T(8,128)S(1)}, f32[32,512]{1,0:T(8,128)}, u32[]{:S(2)}) copy-start(f32[32,512]{1,0:T(8,128)} %param.30) | copy-start | bytes 196612
  170.8 106.7 %copy-start.16 = (f32[32,512]{1,0:T(8,128)S(1)}, f32[32,512]{1,0:T(8,128)}, u32[]{:S(2)}) copy-start(f32[32,512]{1,0:T(8,128)} %param.28) | copy-start | bytes 196612
  170.8 106.7 %copy-start.17 = (f32[32,512]{1,0:T(8,128)S(1)}, f32[32,512]{1,0:T(8,128)}, u32[]{:S(2)}) copy-start(f32[32,512]{1,0:T(8,128)} %param.33) | copy-start | bytes 196612
  170.8 106.8 %copy-start.18 = (f32[32,512]{1,0:T(8,128)S(1)}, f32[32,512]{1,0:T(8,128)}, u32[]{:S(2)}) copy-start(f32[32,512]{1,0:T(8,128)} %param.31) | copy-start | bytes 196612
  170.8 106.8 %copy-start.19 = (f32[32,512]{1,0:T(8,128)S(1)}, f32[32,512]{1,0:T(8,128)}, u32[]{:S(2)}) copy-start(f32[32,512]{1,0:T(8,128)} %param.29) | copy-start | bytes 196612
  170.8 139.7 %copy-start.7 = (bf16[512,256]{1,0:T(8,128)(2,1)S(1)}, bf16[512,256]{1,0:T(8,128)(2,1)}, u32[]{:S(2)}) copy-start(bf16[512,256]{1,0:T(8,128)(2,1)} %param.23) | copy-start | bytes 786436
  170.9 215.8 %all-gather.15.cloned.1.call-start = ((), (), s32[]{:S(2)}) async-start(), calls=%async_computation.6 | async-start | bytes 4718592 | tf_op jit(solution)/shard_map/all_gather | solution.py:97
  235.1 42.5 %copy-start.11 = (f32[32,1536]{1,0:T(8,128)S(1)}, f32[32,1536]{1,0:T(8,128)}, u32[]{:S(2)}) copy-start(f32[32,1536]{1,0:T(8,128)} %reduce-scatter.2.cloned.1.call-done) | copy-start | bytes 589828
  312.0 1.6 copy-start.8
  312.0 149.9 %all-gather.13.cloned.1.call-start = ((), (), s32[]{:S(2)}) async-start(), calls=%async_computation.5 | async-start | bytes 4718592 | tf_op jit(solution)/shard_map/all_gather | solution.py:96
  316.0 2.8 copy-start.10
  316.0 219.1 %all-gather.17.cloned.1.call-start = ((), (), s32[]{:S(2)}) async-start(), calls=%async_computation.7 | async-start | bytes 4718592 | tf_op jit(solution)/shard_map/all_gather | solution.py:98
  330.3 2.6 copy-start.12
  330.3 2.6 copy-start.13
  535.1 6.4 %copy-start.1 = (bf16[1024,512]{1,0:T(8,128)(2,1)S(1)}, bf16[1024,512]{1,0:T(8,128)(2,1)}, u32[]{:S(2)}) copy-start(bf16[1024,512]{1,0:T(8,128)(2,1)} %param.20) | copy-start | bytes 3145732
  (3 other events, 3.5 us)
Sparse Core Ops, SparseCore 0:
  10.1 51.7 all-gather.10
  64.1 47.6 all-gather.8
  113.9 47.6 all-gather.6
  171.0 64.0 reduce-scatter.1
  312.1 74.4 all-gather.14
  389.1 72.8 all-gather.12
  464.1 70.9 all-gather.16
where the time goes:
time: 549 us; the launch traced here: 548 us
  waiting for transfers between devices  390 us (71%)
  blocking collectives  71.8 us (13%)
  local copies, waits for them, and re-layouts  34.9 us (6%)
  matrix products  29.3 us (5%)
  between operations  15.1 us (3%)
  other arithmetic  6.4 us (1%)
    all_gather x1, waiting for transfers between devices, body(): lax.all_gather(query_master_new.astype(jnp.bfloat16), 'fs', axis=0, tiled...  68.9 us
    all_gather x1, waiting for transfers between devices, body(): lax.all_gather(output_master_new.astype(jnp.bfloat16), 'fs', axis=1, tile...  66.7 us
    reduce_scatter x1, waiting for transfers between devices, body(): lax.psum_scatter(partial_value, 'fs', scatter_dimension=0, tiled=True)  64.1 us
    all_gather x1, waiting for transfers between devices, body(): lax.all_gather(key_master_new.astype(jnp.bfloat16), 'fs', axis=0, tiled=T...  53 us
    all_gather x1, waiting for transfers between devices, body(): lax.all_gather(output_basis, 'fs', axis=0, tiled=True)  52.5 us
    all_gather x1, waiting for transfers between devices, body(): lax.all_gather(key_basis, 'fs', axis=0, tiled=True)  42.2 us
    all_gather x1, waiting for transfers between devices, body(): lax.all_gather(query_basis, 'fs', axis=0, tiled=True)  40.7 us
    psum x1, blocking collectives, body(): sum_squares = lax.psum(jnp.sum(shares * shares), ('fs', 'tp'))  39.7 us
  transfers between devices with their start and end apart: 7, of which 7 were waited for; matrix products, arithmetic and copies ran while one was open for 9% of the time, Pallas kernels for 0%

commit v1 on v0

v1 whole, which is shorter than its diff:
```python
import functools
import jax
import jax.numpy as jnp
from jax import lax
from jax.experimental import pallas as pl
from jax.experimental.pallas import tpu as pltpu
from jax.sharding import PartitionSpec as P

RANK = 256
C_W = 2048
MESH = pl.DeviceIdType.MESH

bias_first = 1.0 / (1.0 - 0.8**10)
bias_second = 1.0 / (1.0 - 0.95**10)
learn_rate = 0.05
decay_rate = 0.1


def slot(ref, dim, owner, size, part, rows):
    if ref.ndim == 3:
        return ref.at[owner, pl.ds(part * rows, rows), :]
    if dim == 0:
        return ref.at[pl.ds(pl.multiple_of(owner * size + part * rows, 8), rows), :]
    return ref.at[pl.ds(part * rows, rows), pl.ds(pl.multiple_of(owner * size, 128), size)]


def gather_kernel(axis, major, minor, cut, dims, sizes, *refs):
    arrays = len(dims)
    count = arrays * cut
    whole_ins, outs = refs[:arrays], refs[arrays : 2 * arrays]
    (local, up_send, up_recv, down_send, down_recv, side_send, side_recv, pair_send, pair_recv) = refs[
        2 * arrays :
    ]
    heights = [ref.shape[0] // cut for ref in whole_ins]
    ins = [whole_ins[c // cut].at[pl.ds(c % cut * heights[c // cut], heights[c // cut]), :] for c in range(count)]
    ends = {c for c in range(count) if c % 2 and major >= 4 and major % 2 == 0}
    me = lax.axis_index(axis)
    z, y = me // minor, me % minor

    def side_peer(o):
        return z * minor + (y + o) % minor

    barrier = pltpu.get_barrier_semaphore()

    @pl.when(z < major - 1)
    def _():
        pl.semaphore_signal(barrier, inc=1, device_id={axis: me + minor}, device_id_type=MESH)

    @pl.when(z > 0)
    def _():
        pl.semaphore_signal(barrier, inc=1, device_id={axis: me - minor}, device_id_type=MESH)

    for o in range(1, minor):
        pl.semaphore_signal(barrier, inc=1, device_id={axis: side_peer(o)}, device_id_type=MESH)

    later, earlier = (2 * major - 2 - z) // major, (z + major - 1) // major
    pl.semaphore_wait(barrier, later + earlier + minor - 1)

    def at(c, owner):
        a = c // cut
        return slot(outs[a], dims[a], owner, sizes[a], c % cut, heights[a])

    def line(sign, d, c):
        owner = me - sign * d * minor
        send, recv = (up_send, up_recv) if sign > 0 else (down_send, down_recv)
        return pltpu.make_async_remote_copy(
            src_ref=ins[c] if d == 0 else at(c, owner),
            dst_ref=at(c, owner),
            send_sem=send.at[d, c],
            recv_sem=recv.at[d, c],
            device_id={axis: me + sign * minor},
            device_id_type=MESH,
        )

    def line_arrival(sign, d, c):
        owner = me - sign * d * minor
        send, recv = (up_send, up_recv) if sign > 0 else (down_send, down_recv)
        return pltpu.make_async_remote_copy(
            src_ref=at(c, owner),
            dst_ref=at(c, owner),
            send_sem=send.at[d - 1, c],
            recv_sem=recv.at[d - 1, c],
            device_id={axis: me - sign * minor},
            device_id_type=MESH,
        )

    def side(sign, d, o, c):
        owner = me - sign * d * minor
        index = d if sign > 0 else major + d
        return pltpu.make_async_remote_copy(
            src_ref=ins[c] if d == 0 else at(c, owner),
            dst_ref=at(c, owner),
            send_sem=side_send.at[index, o, c],
            recv_sem=side_recv.at[index, o, c],
            device_id={axis: side_peer(o)},
            device_id_type=MESH,
        )

    def side_arrival(sign, d, o, c):
        source = (y + minor - o) % minor
        owner = (z - sign * d) * minor + source
        index = d if sign > 0 else major + d
        return pltpu.make_async_remote_copy(
            src_ref=at(c, owner),
            dst_ref=at(c, owner),
            send_sem=side_send.at[index, o, c],
            recv_sem=side_recv.at[index, o, c],
            device_id={axis: side_peer(o)},
            device_id_type=MESH,
        )

    def takes(sign):
        return z % 2 == (1 if sign > 0 else 0)

    def gives(sign):
        return z % 2 == (0 if sign > 0 else 1)

    def to_pair(sign, o, c):
        owner = z * minor + (y + minor - o) % minor
        return pltpu.make_async_remote_copy(
            src_ref=at(c, owner),
            dst_ref=at(c, owner),
            send_sem=pair_send.at[o, c],
            recv_sem=pair_recv.at[o, c],
            device_id={axis: me + sign * minor},
            device_id_type=MESH,
        )

    def pair_arrival(sign, o, c):
        owner = (z - sign) * minor + (y + minor - o) % minor
        return pltpu.make_async_remote_copy(
            src_ref=at(c, owner),
            dst_ref=at(c, owner),
            send_sem=pair_send.at[o, c],
            recv_sem=pair_recv.at[o, c],
            device_id={axis: me - sign * minor},
            device_id_type=MESH,
        )

    def held(sign, d):
        return z >= d if sign > 0 else z + d < major

    def onward(sign):
        return z < major - 1 if sign > 0 else z > 0

    for c in range(count):
        for sign in (1, -1):
            pl.when(onward(sign))(line(sign, 0, c).start)
        for o in range(1, minor):
            side(1, 0, o, c).start()
    for c in range(count):
        pltpu.make_async_copy(ins[c], at(c, me), local.at[c]).start()
    for d in range(1, major):
        for c in range(count):
            for sign in (1, -1):

                @pl.when(held(sign, d))
                def _(sign=sign, d=d, c=c):
                    line_arrival(sign, d, c).wait_recv()
                    if d < major - 1:
                        pl.when(onward(sign))(line(sign, d, c).start)
                    for o in range(1, minor):
                        if d == 1 and c in ends:
                            pl.when(jnp.logical_not(takes(sign)))(side(sign, d, o, c).start)
                        else:
                            side(sign, d, o, c).start()

            if d == 1 and c in ends:
                for sign in (1, -1):

                    @pl.when(gives(sign))
                    def _(sign=sign, c=c):
                        for o in range(1, minor):
                            side_arrival(1, 0, o, c).wait_recv()
                            to_pair(sign, o, c).start()

    for d in range(major):
        for sign in (1, -1) if d else (1,):

            @pl.when(held(sign, d))
            def _(sign=sign, d=d):
                for c in range(count):
                    for o in range(1, minor):
                        if c in ends and d == 0:
                            pl.when(gives(1))(to_pair(1, o, c).wait_send)
                            pl.when(gives(-1))(to_pair(-1, o, c).wait_send)
                            side(sign, d, o, c).wait_send()
                        elif c in ends and d == 1:

                            @pl.when(jnp.logical_not(takes(sign)))
                            def _(o=o, c=c):
                                side_arrival(sign, d, o, c).wait_recv()
                                side(sign, d, o, c).wait_send()

                            pl.when(takes(sign))(pair_arrival(sign, o, c).wait_recv)
                        else:
                            side_arrival(sign, d, o, c).wait_recv()
                            side(sign, d, o, c).wait_send()

        if d < major - 1:
            for sign in (1, -1):

                @pl.when(jnp.logical_and(held(sign, d), onward(sign)))
                def _(sign=sign, d=d):
                    for c in range(count):
                        line(sign, d, c).wait_send()

    for c in range(count):
        pltpu.make_async_copy(ins[c], at(c, me), local.at[c]).wait()


def gather(axis, n, minor, blocks, outs, dims, space, name):
    major = n // minor
    cut = 2
    arrays = len(blocks)
    count = arrays * cut
    sizes = tuple(b.shape[d] if o.ndim == 2 else 1 for b, o, d in zip(blocks, outs, dims))
    return pl.pallas_call(
        functools.partial(gather_kernel, axis, major, minor, cut, tuple(dims), sizes),
        out_shape=outs,
        in_specs=[pl.BlockSpec(memory_space=pltpu.VMEM)] * arrays,
        out_specs=[pl.BlockSpec(memory_space=space)] * arrays,
        scratch_shapes=[
            pltpu.SemaphoreType.DMA((count,)),
            pltpu.SemaphoreType.DMA((major, count)),
            pltpu.SemaphoreType.DMA((major, count)),
            pltpu.SemaphoreType.DMA((major, count)),
            pltpu.SemaphoreType.DMA((major, count)),
            pltpu.SemaphoreType.DMA((2 * major, minor, count)),
            pltpu.SemaphoreType.DMA((2 * major, minor, count)),
            pltpu.SemaphoreType.DMA((minor, count)),
            pltpu.SemaphoreType.DMA((minor, count)),
        ],
        compiler_params=pltpu.CompilerParams(collective_id=name, has_side_effects=True),
    )(*blocks)


def moment_kernel(n, parts, partial, first, second, first_new, second_new, portion,
                  arrived, squares, part_send, part_recv, square_send, square_recv, way_send, way_recv):
    me, col = lax.axis_index("fs"), lax.axis_index("tp")
    rows = first.shape[0]
    barrier = pltpu.get_barrier_semaphore()
    for k in range(1, n):
        pl.semaphore_signal(barrier, inc=1, device_id={"fs": (me + k) % n}, device_id_type=MESH)
    for k in range(1, parts):
        pl.semaphore_signal(barrier, inc=1, device_id={"tp": (col + k) % parts}, device_id_type=MESH)
    pl.semaphore_wait(barrier, n + parts - 2)

    def share(k):
        target = (me + k) % n
        return pltpu.make_async_remote_copy(
            src_ref=partial.at[pl.ds(pl.multiple_of(target * rows, 8), rows), :],
            dst_ref=arrived.at[k],
            send_sem=part_send.at[k],
            recv_sem=part_recv.at[k],
            device_id={"fs": target},
            device_id_type=MESH,
        )

    def square(axis, position, size, source, base, k):
        return pltpu.make_async_remote_copy(
            src_ref=squares.at[source],
            dst_ref=squares.at[base + k],
            send_sem=square_send.at[base + k],
            recv_sem=square_recv.at[base + k],
            device_id={axis: (position + k) % size},
            device_id_type=MESH,
        )

    for k in range(1, n):
        share(k).start()
    total = partial[pl.ds(pl.multiple_of(me * rows, 8), rows), :].astype(jnp.float32)
    for k in range(1, n):
        share(k).wait_recv()
        total = total + arrived[k].astype(jnp.float32)

    columns = jnp.sum(total * total, axis=0, keepdims=True)
    lanes = columns[:, :128]
    for j in range(1, columns.shape[1] // 128):
        lanes = lanes + columns[:, j * 128 : (j + 1) * 128]
    squares[0] = jnp.broadcast_to(lanes, squares.shape[1:])
    for k in range(1, parts):
        square("tp", col, parts, 0, 0, k).start()
    lanes = squares[0]
    for k in range(1, parts):
        square("tp", col, parts, 0, 0, k).wait_recv()
        lanes = lanes + squares[k]
    squares[parts] = lanes
    for k in range(1, n):
        square("fs", me, n, parts, parts, k).start()
    second_scaled = 0.95 * second[...]
    first_scaled = 0.8 * first[...]
    for k in range(1, n):
        square("fs", me, n, parts, parts, k).wait_recv()
        lanes = lanes + squares[parts + k]
    sum_squares = jnp.sum(lanes[:1], axis=1, keepdims=True)
    clip_factor = jnp.minimum(1.0, jnp.sqrt(3.0 * RANK * C_W / sum_squares))
    clipped = clip_factor * total
    first_value = first_scaled + 0.2 * clipped
    second_value = second_scaled + 0.05 * clipped * clipped
    mine = pl.ds(pl.multiple_of(me * rows, 8), rows)
    portion[mine, :] = (
        first_value * bias_first / (jnp.sqrt(second_value * bias_second) + 1e-08)
    ).astype(jnp.bfloat16)
    first_new[...] = first_value
    second_new[...] = second_value

    def way(k, owner):
        place = pl.ds(pl.multiple_of(owner * rows, 8), rows)
        return pltpu.make_async_remote_copy(
            src_ref=portion.at[place, :],
            dst_ref=portion.at[place, :],
            send_sem=way_send.at[k],
            recv_sem=way_recv.at[k],
            device_id={"fs": (me + k) % n},
            device_id_type=MESH,
        )

    for k in range(1, n):
        way(k, me).start()
    for k in range(1, n):
        share(k).wait_send()
        square("fs", me, n, parts, parts, k).wait_send()
    for k in range(1, parts):
        square("tp", col, parts, 0, 0, k).wait_send()
    for k in range(1, n):
        way(k, (me + n - k) % n).wait_recv()
        way(k, me).wait_send()


def moments(n, parts, partial, first, second):
    rows, width = first.shape
    return pl.pallas_call(
        functools.partial(moment_kernel, n, parts),
        out_shape=[
            jax.ShapeDtypeStruct(first.shape, jnp.float32),
            jax.ShapeDtypeStruct(first.shape, jnp.float32),
            jax.ShapeDtypeStruct(partial.shape, jnp.bfloat16),
        ],
        in_specs=[pl.BlockSpec(memory_space=pltpu.VMEM)] * 3,
        out_specs=[pl.BlockSpec(memory_space=pltpu.VMEM)] * 3,
        scratch_shapes=[
            pltpu.VMEM((n, rows, width), jnp.bfloat16),
            pltpu.VMEM((n + parts, 8, 128), jnp.float32),
            pltpu.SemaphoreType.DMA((n,)),
            pltpu.SemaphoreType.DMA((n,)),
            pltpu.SemaphoreType.DMA((n + parts,)),
            pltpu.SemaphoreType.DMA((n + parts,)),
            pltpu.SemaphoreType.DMA((n,)),
            pltpu.SemaphoreType.DMA((n,)),
        ],
        compiler_params=pltpu.CompilerParams(collective_id=3, has_side_effects=True),
    )(partial, first, second)


def body(
    n,
    parts,
    normed_input,
    query_cotangent,
    key_cotangent,
    head_outputs,
    output_cotangent,
    query_basis,
    key_basis,
    output_basis,
    query_master,
    key_master,
    output_master,
    query_first,
    query_second,
    key_first,
    key_second,
    output_first,
    output_second,
):
    width = query_cotangent.shape[1]
    tokens, depth = normed_input.shape
    bases = (query_basis, key_basis, output_basis)
    rank = query_basis.shape[1]
    piece = rank // parts
    minor = n // 4 if n % 4 == 0 else 1
    place = lax.axis_index("tp") * piece
    mine = jnp.concatenate(
        [lax.dynamic_slice_in_dim(b, place, piece, axis=1).T for b in bases], axis=0
    )
    (basis_rows,) = gather(
        "fs", n, minor, [mine], [jax.ShapeDtypeStruct((3 * piece, depth), jnp.bfloat16)], [1],
        pltpu.VMEM, 1,
    )
    contract = (((1,), (1,)), ((), ()))
    reduced = jnp.concatenate(
        [
            lax.dot_general(basis_rows[: 2 * piece], normed_input, contract,
                            preferred_element_type=jnp.float32),
            lax.dot_general(basis_rows[2 * piece :], output_cotangent, contract,
                            preferred_element_type=jnp.float32),
        ],
        axis=0,
    ).astype(jnp.bfloat16)
    (every,) = gather(
        "tp", parts, 2 if parts % 2 == 0 else 1, [reduced],
        [jax.ShapeDtypeStruct((parts, 3 * piece, tokens), jnp.bfloat16)], [0], pltpu.VMEM, 2,
    )
    right_sides = (query_cotangent, key_cotangent, head_outputs)
    partial_value = jnp.concatenate(
        [
            jnp.dot(
                every[:, member * piece : (member + 1) * piece].reshape(rank, tokens),
                right_sides[member],
                preferred_element_type=jnp.float32,
            ).astype(jnp.bfloat16)
            for member in range(3)
        ],
        axis=1,
    )
    first_moment = jnp.concatenate([query_first, key_first, output_first], axis=1)
    second_moment = jnp.concatenate([query_second, key_second, output_second], axis=1)
    first_new, second_new, portion = moments(n, parts, partial_value, first_moment, second_moment)
    query_update = 0.25 * jnp.dot(
        query_basis, portion[:, :width], preferred_element_type=jnp.float32
    )
    key_update = 0.25 * jnp.dot(
        key_basis, portion[:, width : 2 * width], preferred_element_type=jnp.float32
    )
    output_update = 0.25 * lax.dot_general(
        portion[:, 2 * width :], output_basis, (((0,), (1,)), ((), ())),
        preferred_element_type=jnp.float32,
    )
    query_master_new = query_master - learn_rate * (query_update + decay_rate * query_master)
    key_master_new = key_master - learn_rate * (key_update + decay_rate * key_master)
    output_master_new = output_master - learn_rate * (output_update + decay_rate * output_master)
    query_copy, key_copy, output_copy = gather(
        "fs", n, minor,
        [v.astype(jnp.bfloat16) for v in (query_master_new, key_master_new, output_master_new)],
        [
            jax.ShapeDtypeStruct((depth, width), jnp.bfloat16),
            jax.ShapeDtypeStruct((depth, width), jnp.bfloat16),
            jax.ShapeDtypeStruct((width, depth), jnp.bfloat16),
        ],
        [0, 0, 1], pl.ANY, 4,
    )
    return (
        query_master_new,
        key_master_new,
        output_master_new,
        query_copy,
        key_copy,
        output_copy,
        query_update.astype(jnp.bfloat16),
        key_update.astype(jnp.bfloat16),
        output_update.astype(jnp.bfloat16),
        first_new[:, :width],
        second_new[:, :width],
        first_new[:, width : 2 * width],
        second_new[:, width : 2 * width],
        first_new[:, 2 * width :],
        second_new[:, 2 * width :],
    )


def solution(mesh):
    placed = (
        P("fs", None),
        P("fs", "tp"),
        P("fs", "tp"),
        P("fs", "tp"),
        P("fs", None),
        P("fs", None),
        P("fs", None),
        P("fs", None),
        P("fs", "tp"),
        P("fs", "tp"),
        P("tp", "fs"),
        P("fs", "tp"),
        P("fs", "tp"),
        P("fs", "tp"),
        P("fs", "tp"),
        P("fs", "tp"),
        P("fs", "tp"),
    )
    return jax.shard_map(
        functools.partial(body, mesh.shape["fs"], mesh.shape["tp"]),
        mesh=mesh,
        in_specs=placed,
        out_specs=(
            P("fs", "tp"),
            P("fs", "tp"),
            P("tp", "fs"),
            P(None, "tp"),
            P(None, "tp"),
            P("tp", None),
            P("fs", "tp"),
            P("fs", "tp"),
            P("tp", "fs"),
            P("fs", "tp"),
            P("fs", "tp"),
            P("fs", "tp"),
            P("fs", "tp"),
            P("fs", "tp"),
            P("fs", "tp"),
        ),
        check_vma=False,
    )
```

time: 549 us -> 273 us (0.50)
  waiting for transfers between devices: 390 us -> 0 us
  Pallas kernels: 0 us -> 222 us
  blocking collectives: 71.8 us -> 0 us
  between operations: 15.1 us -> 0.89 us
  local copies, waits for them, and re-layouts: 34.9 us -> 23.9 us
  matrix products: 29.3 us -> 19.5 us
    all_gather x6 -> x0, waiting for transfers between devices: 324 us -> none  [the longest x1 68.9 us: body(): lax.all_gather(query_master_new.astype(jnp.bfloat16), 'fs', axis=0, tiled...]
    pallas_call x0 -> x4, Pallas kernels: none -> 222 us  [the longest x3 179 us: gather(): pl.pallas_call(functools.partial(gather_kernel, axis, major, minor, cut,...]
    reduce_scatter x1 -> x0, waiting for transfers between devices: 64.1 us -> none  [body(): lax.psum_scatter(partial_value, 'fs', scatter_dimension=0, tiled=True)]
    psum x1 -> x0, blocking collectives: 39.7 us -> none  [body(): sum_squares = lax.psum(jnp.sum(shares * shares), ('fs', 'tp'))]
    all_gather x1 -> x0, blocking collectives: 32.1 us -> none  [body(): portion = lax.all_gather(direction, 'fs', axis=0, tiled=True)]
    unnamed x51 -> x32, local copies, waits for them, and re-layouts: 32.8 us -> 15.6 us
    dot_general x12 -> x8, matrix products: 29.3 us -> 19.5 us  [the longest x1 6.33 us: body(): lax.dot_general(basis_rows[:2 * piece], normed_input, contract, preferred...]
  transfers between devices with their start and end apart: 7 -> 0, of which waited for: 7 -> 0; matrix products, arithmetic and copies ran while one was open for 9% -> 0% of each run, Pallas kernels for 0% -> 0%
where the time goes in v1:
time: 273 us; the launch traced here: 272 us
  Pallas kernels  222 us (81%)
  local copies, waits for them, and re-layouts  23.9 us (9%)
  matrix products  19.5 us (7%)
  other arithmetic  5.57 us (2%)
    pallas_call x3, Pallas kernels, gather(): pl.pallas_call(functools.partial(gather_kernel, axis, major, minor, cut,...  179 us
    pallas_call x1, Pallas kernels, moments(): pl.pallas_call(functools.partial(moment_kernel, n, parts), out_shape=[jax...  43.4 us
    unnamed x32, local copies, waits for them, and re-layouts  15.6 us
    dot_general x1, matrix products, body(): lax.dot_general(basis_rows[:2 * piece], normed_input, contract, preferred...  6.33 us
    dot_general x1, matrix products, body(): lax.dot_general(basis_rows[2 * piece:], output_cotangent, contract, prefe...  6.31 us

profile of v1, /device:TPU:0, one launch (start us, length us, event | category | flops | bytes accessed | tf_op | source)
XLA Modules:
  0.0 272.1 jit_solution(17926209896984564647)
XLA Ops:
  0.7 1.1 constant_dynamic-slice_fusion.2
  1.9 1.1 constant_dynamic-slice_fusion
  3.9 1.8 pad_maximum_fusion.3
  5.7 1.6 copy.38
  7.2 27.3 %shard_map.280 = bf16[192,4096]{1,0:T(8,128)(2,1)} custom-call(bf16[192,512]{1,0:T(8,128)(2,1)} %pad_maximum_fusion.2.refs_0_), custom_call_target="tpu_custom_call" | custom-call | tf_op jit(solution)/shard_map/pallas_call | solution.py:218
  34.5 6.3 %convolution_convert_fusion.4 = bf16[64,1024]{1,0:T(8,128)(2,1)S(1)} fusion(bf16[1024,4096]{1,0:T(8,128)(2,1)} %param.21, bf16[192,4096]{1,0:T(8,128)(2,1)} %shard_map.280), kind=kOutput, calls=%fused_computation.9 | convolution fusion | flops 536936448 | bytes 9043968 | tf_op jit(solution)/shard_map/dot_general | solution.py:396
  40.8 6.3 %convolution_convert_fusion.3 = bf16[128,1024]{1,0:T(8,128)(2,1)S(1)} fusion(bf16[1024,4096]{1,0:T(8,128)(2,1)} %param.17, bf16[192,4096]{1,0:T(8,128)(2,1)S(1)} %copy-done.2), kind=kOutput, calls=%fused_computation.8 | convolution fusion | flops 1073872896 | bytes 9699328 | tf_op jit(solution)/shard_map/dot_general | solution.py:394
  48.0 15.0 %shard_map.281 = bf16[4,192,1024]{2,1,0:T(8,128)(2,1)} custom-call(bf16[192,1024]{1,0:T(8,128)(2,1)} %pad_maximum_fusion.1.refs_0_), custom_call_target="tpu_custom_call" | custom-call | tf_op jit(solution)/shard_map/pallas_call | solution.py:218
  63.0 1.6 fusion.10
  67.0 43.4 %shard_map.282 = (f32[32,1536]{1,0:T(8,128)}, f32[32,1536]{1,0:T(8,128)}, bf16[256,1536]{1,0:T(8,128)(2,1)}) custom-call(bf16[256,1536]{1,0:T(8,128)(2,1)} %pad_maximum_fusion.partial, f32[32,1536]{1,0:T(8,128)} %get-tuple-element.65.first, f32[32,1536]{1,0:T(8,128)} %get-tuple-element.66.second), custom_call_target="tpu_custom_call" | custom-call | tf_op jit(solution)/shard_map/pallas_call | solution.py:333
  110.4 1.6 fusion.12
  112.0 1.6 fusion.11
  113.6 1.4 fusion.9
  114.9 1.0 copy.40.refs_0_
  117.0 1.3 copy.41
  118.3 1.4 fusion.13
  119.7 1.0 copy.43
  121.1 1.4 fusion.8
  122.5 2.7 fusion.7
  125.2 136.6 %shard_map.283 = (bf16[4096,512]{1,0:T(8,128)(2,1)}, bf16[4096,512]{1,0:T(8,128)(2,1)}, bf16[512,4096]{1,0:T(8,128)(2,1)}) custom-call(bf16[512,512]{1,0:T(8,128)(2,1)} %copy.40.refs_0_, bf16[512,512]{1,0:T(8,128)(2,1)} %get-tuple-element.44.refs_1_, bf16[512,512]{1,0:T(8,128)(2,1)} %get-tuple-element.42.refs_2_), custom_call_target="tpu_custom_call" | custom-call | tf_op jit(solution)/shard_map/pallas_call | solution.py:218
  261.8 4.6 %copy.50 = bf16[4096,512]{1,0:T(8,128)(2,1)} copy(bf16[4096,512]{1,0:T(8,128)(2,1)} %get-tuple-element.85) | data formatting | bytes 8388608
  266.4 2.1 copy.51
  268.5 1.6 copy-done.3
  270.1 2.0 copy.52
  (32 shorter events, 5.4 us)
Async XLA Ops:
  0.6 64.0 %copy-start = (bf16[1024,512]{1,0:T(8,128)(2,1)S(1)}, bf16[1024,512]{1,0:T(8,128)(2,1)}, u32[]{:S(2)}) copy-start(bf16[1024,512]{1,0:T(8,128)(2,1)} %param.18) | copy-start | bytes 3145732
  34.5 6.3 %copy-start.2 = (bf16[192,4096]{1,0:T(8,128)(2,1)S(1)}, bf16[192,4096]{1,0:T(8,128)(2,1)}, u32[]{:S(2)}) copy-start(bf16[192,4096]{1,0:T(8,128)(2,1)} %shard_map.280) | copy-start | bytes 4718596
  47.2 17.9 %copy-start.7 = (bf16[1024,512]{1,0:T(8,128)(2,1)S(1)}, bf16[1024,512]{1,0:T(8,128)(2,1)}, u32[]{:S(2)}) copy-start(bf16[1024,512]{1,0:T(8,128)(2,1)} %param.20) | copy-start | bytes 3145732
  63.0 2.6 copy-start.8
  64.6 48.9 %copy-start.10 = (bf16[512,256]{1,0:T(8,128)(2,1)S(1)}, bf16[512,256]{1,0:T(8,128)(2,1)}, u32[]{:S(2)}) copy-start(bf16[512,256]{1,0:T(8,128)(2,1)} %param.22) | copy-start | bytes 786436
  117.0 4.1 %copy-start.5 = (f32[512,512]{1,0:T(8,128)S(1)}, f32[512,512]{1,0:T(8,128)}, u32[]{:S(2)}) copy-start(f32[512,512]{1,0:T(8,128)} %param.26) | copy-start | bytes 3145732
  118.3 4.2 %copy-start.9 = (bf16[512,256]{1,0:T(8,128)(2,1)S(1)}, bf16[512,256]{1,0:T(8,128)(2,1)}, u32[]{:S(2)}) copy-start(bf16[512,256]{1,0:T(8,128)(2,1)} %param.24) | copy-start | bytes 786436
  121.1 1.4 copy-start.6
  261.7 4.6 %copy-start.4 = (bf16[4096,512]{1,0:T(8,128)(2,1)S(1)}, bf16[4096,512]{1,0:T(8,128)(2,1)}, u32[]{:S(2)}) copy-start(bf16[4096,512]{1,0:T(8,128)(2,1)} %get-tuple-element.86) | copy-start | bytes 12582916
  266.4 3.7 %copy-start.3 = (bf16[512,4096]{1,0:T(8,128)(2,1)S(1)}, bf16[512,4096]{1,0:T(8,128)(2,1)}, u32[]{:S(2)}) copy-start(bf16[512,4096]{1,0:T(8,128)(2,1)} %get-tuple-element.87) | copy-start | bytes 12582916
  266.4 5.7 %copy-start.1 = (bf16[1024,512]{1,0:T(8,128)(2,1)S(1)}, bf16[1024,512]{1,0:T(8,128)(2,1)}, u32[]{:S(2)}) copy-start(bf16[1024,512]{1,0:T(8,128)(2,1)} %param.18) | copy-start | bytes 3145732
